TPU v7x, 32 devices: a whole 2x2x4 slice. The times are simulated.
32 devices in a mesh: fs: 4 (over z), rep: 4 (over y, x), tp: 2 (over core).
Axes of the slice: x: 2, y: 2, z: 4, core: 2. Of those that a mesh axis runs over, the one named last changes fastest.
Arguments:
- normed: bfloat16 [10240, 2048], P(('fs', 'rep')), may hold values from -150 to 150
- rec_cot: bfloat16 [10240, 2048], P(('fs', 'rep'), 'tp'), may hold values from -1.4823177 to 1.4823177
- conv_out: bfloat16 [10240, 2048], P(('fs', 'rep'), 'tp'), may hold values from -6 to 6
- gate_cot: bfloat16 [10240, 2048], P(('fs', 'rep'), 'tp'), may hold values from -0.05908203 to 0.05908203
- rec_weight: float32 [2048, 2048], P('fs', 'tp'), may hold values from -0.125 to 0.125
- rec_moment: float32 [2048, 2048], P('fs', 'tp'), may hold values from -6 to 6
- rec_right: bfloat16 [2048, 256], P('tp'), may hold values from -1 to 2
- gate_weight: float32 [8, 256, 256], P('tp', 'fs'), may hold values from -0.375 to 0.375
- gate_moment: float32 [8, 256, 256], P('tp', 'fs'), may hold values from -6 to 6
- gate_left: bfloat16 [8, 256, 256], P('tp', 'fs'), may hold values from -1 to 2
- gate_right: bfloat16 [8, 256, 256], P('tp'), may hold values from -1 to 2
Outputs:
- rec_weight_new: float32 [2048, 2048], P('fs', 'tp')
- rec_moment_new: float32 [2048, 2048], P('fs', 'tp')
- rec_step: float32 [2048, 2048], P('fs', 'tp')
- rec_copy: bfloat16 [2048, 2048], P('fs', 'tp')
- gate_weight_new: float32 [8, 256, 256], P('tp', 'fs')
- gate_moment_new: float32 [8, 256, 256], P('tp', 'fs')
- gate_step: float32 [8, 256, 256], P('tp', 'fs')
- gate_copy: bfloat16 [8, 256, 256], P('tp', 'fs')
All inputs are finite; a program needn't handle non-finite values.
Results may differ from a plain program's by a relative error of at most 0.001.
Values sent between devices are 32-bit elements; how exact they have to be, the bound alone decides.
A program may use at most 64 MiB of HBM per device.

v0:
```python
import functools

import jax
import jax.numpy as jnp
from jax import lax
from jax.experimental import pallas as pl
from jax.experimental.pallas import tpu as pltpu
from jax.sharding import PartitionSpec as P

BETA = 0.9
LEARN_RATE = 0.02
EPSILON = 1e-06
MESH = pl.DeviceIdType.MESH
LANES = 128


def split_dot(value, factor):
    high = value.astype(jnp.bfloat16)
    low = (value - high.astype(jnp.float32)).astype(jnp.bfloat16)
    return jnp.dot(high, factor, preferred_element_type=jnp.float32) + jnp.dot(
        low, factor, preferred_element_type=jnp.float32
    )


def split_dot_left(factor, value):
    high = value.astype(jnp.bfloat16)
    low = (value - high.astype(jnp.float32)).astype(jnp.bfloat16)
    return jnp.dot(factor, high, preferred_element_type=jnp.float32) + jnp.dot(
        factor, low, preferred_element_type=jnp.float32
    )


def token_dot(left, right):
    return lax.dot_general(left, right, (((0,), (0,)), ((), ())), preferred_element_type=jnp.float32)


def folded_squares(value):
    squares = value * value
    rows, width = squares.shape
    total = jnp.sum(squares.reshape(rows // 8, 8, width), axis=0)
    result = total[:, :LANES]
    for start in range(LANES, width, LANES):
        result = result + total[:, start : start + LANES]
    return result


def kernel(
    fs_size, tp_size, halves,
    normed, rec_cot, conv_out, gate_cot, rec_moment, rec_right, gate_moment, gate_left, gate_right,
    rec_pre, gate_pre, scales,
    part, first, second, along, grad,
    gate_part, gate_first, gate_second, gate_along, gate_grad,
    sums, sums_fs, sums_tp,
    pair_send, pair_recv, fs_send, fs_recv, sum_send, sum_recv,
):
    fs, rep, tp = lax.axis_index("fs"), lax.axis_index("rep"), lax.axis_index("tp")
    bits = (lax.rem(rep, 2), rep // 2)
    partners = (rep + 1 - 2 * bits[0], rep + 2 - 4 * bits[1])
    fs_peers = [lax.rem(fs + step, fs_size) for step in range(1, fs_size)]
    tp_peers = [lax.rem(tp + step, tp_size) for step in range(1, tp_size)]

    barrier = pltpu.get_barrier_semaphore()
    peers = [{"rep": p} for p in partners] + [{"fs": p} for p in fs_peers] + [{"tp": p} for p in tp_peers]
    for peer in peers:
        pl.semaphore_signal(barrier, inc=1, device_id=peer, device_id_type=MESH)

    chunks = part.shape[0]
    width = part.shape[-1]
    quarter = part.shape[-2]
    half_rows = 8 * quarter
    fs_rows = halves * half_rows
    blocks = gate_part.shape[3]
    gate_rows = gate_part.shape[4]
    unit_count = chunks + 1
    sums[...] = jnp.zeros_like(sums)

    def remote(source, target, send, recv, peer):
        return pltpu.make_async_remote_copy(
            src_ref=source, dst_ref=target, send_sem=send, recv_sem=recv,
            device_id=peer, device_id_type=MESH,
        )

    def views(unit):
        if unit == 0:
            return gate_part, gate_first, gate_second, gate_along, gate_grad
        k = unit - 1
        return part.at[k], first.at[k], second.at[k], along.at[k], grad.at[k]

    def mine(stream):
        return bits[stream], bits[1 - stream]

    def pair_copy(unit, stream, stage):
        p, one, two, _, g = views(unit)
        a, b = mine(stream)
        side = stream if stage in (0, 3) else 1 - stream
        if stage == 0:
            source, target = p.at[stream, 1 - a], one.at[stream]
        elif stage == 1:
            source, target = p.at[stream, a, 1 - b], two.at[stream]
        elif stage == 2:
            source = target = g.at[stream, a, b]
        else:
            source = target = g.at[stream, a]
        return remote(
            source, target, pair_send.at[unit, stream, stage], pair_recv.at[unit, stream, stage],
            {"rep": partners[side]},
        )

    def fs_copy(unit, stream, step):
        p, _, _, slots, _ = views(unit)
        a, b = mine(stream)
        peer = fs_peers[step]
        source = p.at[stream, a, b] if unit == 0 else p.at[stream, a, b, peer]
        return remote(
            source, slots.at[stream, step],
            fs_send.at[unit, stream, step], fs_recv.at[unit, stream, step], {"fs": peer},
        )

    def product(unit):
        if unit == 0:
            @pl.loop(0, blocks)
            def _(block):
                columns = pl.ds(pl.multiple_of(block * width, width), width)
                term = token_dot(conv_out[:, columns], gate_cot[:, columns])
                gate_part[:, :, :, block] = term.reshape(2, 2, 2, gate_rows, width)
        else:
            k = unit - 1
            column, half = k // halves, k % halves
            @pl.loop(0, fs_size)
            def _(owner):
                start = pl.multiple_of(owner * fs_rows + half * half_rows, half_rows)
                term = token_dot(
                    normed[:, pl.ds(start, half_rows)], rec_cot[:, column * width : (column + 1) * width]
                )
                part[k, :, :, :, owner] = term.reshape(2, 2, 2, quarter, width)

    def start_pair(unit, stage):
        for stream in range(2):
            pair_copy(unit, stream, stage).start()

    def add_first(unit):
        p, one, _, _, _ = views(unit)
        for stream in range(2):
            pair_copy(unit, stream, 0).wait_recv()
            a, b = mine(stream)
            @pl.loop(0, p.shape[3])
            def _(i):
                for other in range(2):
                    p[stream, a, other, i] += one[stream, other, i]
            pair_copy(unit, stream, 1).start()

    def add_second(unit):
        p, _, two, _, _ = views(unit)
        for stream in range(2):
            pair_copy(unit, stream, 1).wait_recv()
            a, b = mine(stream)
            @pl.loop(0, p.shape[3])
            def _(i):
                p[stream, a, b, i] += two[stream, i]
            for step in range(fs_size - 1):
                fs_copy(unit, stream, step).start()

    def add_along(unit):
        p, _, _, slots, g = views(unit)
        for stream in range(2):
            a, b = mine(stream)
            for step in range(fs_size - 1):
                fs_copy(unit, stream, step).wait_recv()
            total = p[stream, a, b] if unit == 0 else p[stream, a, b, fs]
            for step in range(fs_size - 1):
                total = total + slots[stream, step]
            g[stream, a, b] = total
            pair_copy(unit, stream, 2).start()

    def forward(unit):
        for stream in range(2):
            pair_copy(unit, stream, 2).wait_recv()
            pair_copy(unit, stream, 3).start()

    def finish(unit):
        for stream in range(2):
            pair_copy(unit, stream, 3).wait_recv()
        if unit == 0:
            @pl.loop(0, blocks)
            def _(block):
                gradient = gate_grad[:, :, :, block].reshape(8 * gate_rows, width)
                right_done = split_dot(gradient, gate_right[block])
                pre = split_dot_left(gate_left[block], right_done)
                gate_pre[block] = pre
                moment = BETA * gate_moment[block] + pre
                sums[2] += folded_squares(gradient) * (1.0 / fs_size)
                sums[3] += folded_squares(moment)
        else:
            k = unit - 1
            column, half = k // halves, k % halves
            columns = slice(column * width, (column + 1) * width)
            rows = slice(half * half_rows, (half + 1) * half_rows)
            gradient = grad[k].reshape(half_rows, width)
            pre = split_dot(gradient, rec_right[columns, :])
            rec_pre[rows, columns] = pre
            moment = BETA * rec_moment[rows, columns] + pre
            sums[0] += folded_squares(gradient)
            sums[1] += folded_squares(moment)

    product(0)
    pl.semaphore_wait(barrier, len(peers))
    stages = (None, add_first, add_second, add_along, forward, finish)
    for tick in range(unit_count + 5):
        if tick < unit_count:
            if tick > 0:
                product(tick)
            start_pair(tick, 0)
        for lag in range(1, 6):
            if 0 <= tick - lag < unit_count:
                stages[lag](tick - lag)

    def exchange(slots, axis, axis_peers, base):
        copies = [
            remote(sums, slots.at[i], sum_send.at[base + i], sum_recv.at[base + i], {axis: peer})
            for i, peer in enumerate(axis_peers)
        ]
        for copy in copies:
            copy.start()
        for copy in copies:
            copy.wait()
        total = sums[...]
        for i in range(len(copies)):
            total = total + slots[i]
        return total

    sums[...] = exchange(sums_fs, "fs", fs_peers, 0)
    total = exchange(sums_tp, "tp", tp_peers, fs_size - 1)
    squares = [jnp.sum(total[i], keepdims=True) for i in range(4)]
    rec_scale = jnp.sqrt(squares[0]) / jnp.sqrt(squares[1] + EPSILON)
    gate_scale = jnp.sqrt(squares[2]) / jnp.sqrt(squares[3] + EPSILON)
    scales[0] = jnp.broadcast_to(rec_scale, (8, LANES))
    scales[1] = jnp.broadcast_to(gate_scale, (8, LANES))

    for unit in range(unit_count):
        for stream in range(2):
            for stage in range(4):
                pair_copy(unit, stream, stage).wait_send()
            for step in range(fs_size - 1):
                fs_copy(unit, stream, step).wait_send()


def shards(fs_size, rep_size, tp_size, normed, rec_cot, conv_out, gate_cot, rec_weight, rec_moment,
           rec_right, gate_weight, gate_moment, gate_left, gate_right):
    assert rep_size == 4
    f32 = jnp.float32
    fs_rows, columns = rec_weight.shape
    width = rec_right.shape[1]
    blocks = gate_weight.shape[0]
    halves = 2 if fs_rows % 256 == 0 else 1
    chunks = columns // width * halves
    quarter = fs_rows // (8 * halves)
    gate_rows = gate_right.shape[1] // 8
    units = chunks + 1
    others = fs_size - 1
    vmem = pl.BlockSpec(memory_space=pltpu.VMEM)
    rec_pre, gate_pre, scales = pl.pallas_call(
        functools.partial(kernel, fs_size, tp_size, halves),
        out_shape=(
            jax.ShapeDtypeStruct(rec_weight.shape, f32),
            jax.ShapeDtypeStruct(gate_weight.shape, f32),
            jax.ShapeDtypeStruct((2, 8, LANES), f32),
        ),
        in_specs=[vmem] * 9,
        out_specs=(vmem,) * 3,
        scratch_shapes=[
            pltpu.VMEM((chunks, 2, 2, 2, fs_size, quarter, width), f32),
            pltpu.VMEM((chunks, 2, 2, fs_size, quarter, width), f32),
            pltpu.VMEM((chunks, 2, fs_size, quarter, width), f32),
            pltpu.VMEM((chunks, 2, others, quarter, width), f32),
            pltpu.VMEM((chunks, 2, 2, 2, quarter, width), f32),
            pltpu.VMEM((2, 2, 2, blocks, gate_rows, width), f32),
            pltpu.VMEM((2, 2, blocks, gate_rows, width), f32),
            pltpu.VMEM((2, blocks, gate_rows, width), f32),
            pltpu.VMEM((2, others, blocks, gate_rows, width), f32),
            pltpu.VMEM((2, 2, 2, blocks, gate_rows, width), f32),
            pltpu.VMEM((4, 8, LANES), f32),
            pltpu.VMEM((others, 4, 8, LANES), f32),
            pltpu.VMEM((tp_size - 1, 4, 8, LANES), f32),
            pltpu.SemaphoreType.DMA((units, 2, 4)),
            pltpu.SemaphoreType.DMA((units, 2, 4)),
            pltpu.SemaphoreType.DMA((units, 2, others)),
            pltpu.SemaphoreType.DMA((units, 2, others)),
            pltpu.SemaphoreType.DMA((others + tp_size - 1,)),
            pltpu.SemaphoreType.DMA((others + tp_size - 1,)),
        ],
        compiler_params=pltpu.CompilerParams(
            collective_id=0, has_side_effects=True, vmem_limit_bytes=60 * 1024 * 1024
        ),
    )(normed, rec_cot, conv_out, gate_cot, rec_moment, rec_right, gate_moment, gate_left, gate_right)

    def update(weight, moment, pre, scale):
        moment_new = BETA * moment + pre
        taken = LEARN_RATE * scale * moment_new
        new = weight - taken
        return new, moment_new, taken, new.astype(jnp.bfloat16)

    return update(rec_weight, rec_moment, rec_pre, scales[0, 0, 0]) + update(
        gate_weight, gate_moment, gate_pre, scales[1, 0, 0]
    )


def solution(mesh):
    in_specs = (
        P(("fs", "rep"), None),
        P(("fs", "rep"), "tp"),
        P(("fs", "rep"), "tp"),
        P(("fs", "rep"), "tp"),
        P("fs", "tp"),
        P("fs", "tp"),
        P("tp", None),
        P("tp", "fs", None),
        P("tp", "fs", None),
        P("tp", "fs", None),
        P("tp", None, None),
    )
    out_specs = (P("fs", "tp"),) * 4 + (P("tp", "fs", None),) * 4
    body = functools.partial(shards, mesh.shape["fs"], mesh.shape["rep"], mesh.shape["tp"])
    return jax.shard_map(body, mesh=mesh, in_specs=in_specs, out_specs=out_specs, check_vma=False)
```

profile of v0, /device:TPU:0, one launch (start us, length us, event | category | flops | bytes accessed | tf_op | source)
XLA Modules:
  0.0 144.8 jit_solution(9501858258850238661)
XLA Ops:
  0.6 0.0 copy-start
  0.6 134.3 %shard_map.170 = (f32[512,1024]{1,0:T(8,128)}, f32[4,64,256]{2,1,0:T(8,128)}, f32[2,8,128]{2,1,0:T(8,128)}) custom-call(bf16[640,2048]{1,0:T(8,128)(2,1)} %normed.1, bf16[640,1024]{1,0:T(8,128)(2,1)} %rec_cot.1, bf16[640,1024]{1,0:T(8,128)(2,1)} %conv_out.1, bf16[640,1024]{1,0:T(8,128)(2,1)} %gate_cot.1, f32[512,1024]{1,0:T(8,128)} %rec_moment.1, ...), custom_call_target="tpu_custom_call" | custom-call | tf_op jit(solution)/shard_map/pallas_call | solution.py:261
  134.9 1.2 fusion.2
  136.8 0.0 copy-done
  136.8 0.0 copy-start.1
  136.8 0.0 copy-start.2
  136.8 0.0 copy-start.3
  136.8 6.3 %fusion.1 = (bf16[512,1024]{1,0:T(8,128)(2,1)}, f32[512,1024]{1,0:T(8,128)}, f32[512,1024]{1,0:T(8,128)}, f32[512,1024]{1,0:T(8,128)}) fusion(f32[512,1024]{1,0:T(8,128)} %param.15, f32[]{:T(128)} %bitcast, f32[512,1024]{1,0:T(8,128)} %get-tuple-element.12, f32[512,1024]{1,0:T(8,128)S(1)} %copy-done), kind=kLoop, calls=%fused_computation.5 | loop fusion | flops 2621440 | bytes 13631492 | tf_op jit(solution)/shard_map/convert_element_type | solution.py:300
  143.8 0.0 copy-done.1
  143.8 0.0 copy-done.2
  143.8 0.0 copy-done.3
  143.8 1.0 fusion
Async XLA Ops:
  0.6 136.2 %copy-start = (f32[512,1024]{1,0:T(8,128)S(1)}, f32[512,1024]{1,0:T(8,128)}, u32[]{:S(2)}) copy-start(f32[512,1024]{1,0:T(8,128)} %rec_moment.1) | copy-start | bytes 6291460
  136.8 7.0 %copy-start.1 = (f32[4,64,256]{2,1,0:T(8,128)S(1)}, f32[4,64,256]{2,1,0:T(8,128)}, u32[]{:S(2)}) copy-start(f32[4,64,256]{2,1,0:T(8,128)} %gate_moment.1) | copy-start | bytes 786436
  136.8 7.0 %copy-start.2 = (f32[4,64,256]{2,1,0:T(8,128)S(1)}, f32[4,64,256]{2,1,0:T(8,128)}, u32[]{:S(2)}) copy-start(f32[4,64,256]{2,1,0:T(8,128)} %param.18) | copy-start | bytes 786436
  136.8 7.0 %copy-start.3 = (f32[4,64,256]{2,1,0:T(8,128)S(1)}, f32[4,64,256]{2,1,0:T(8,128)}, u32[]{:S(2)}) copy-start(f32[4,64,256]{2,1,0:T(8,128)} %get-tuple-element.13) | copy-start | bytes 786436
where the time goes:
time: 145 us
  Pallas kernels  134 us (92%)
  other arithmetic  7.26 us (5%)
  between operations  2.01 us (1%)
    pallas_call x1, Pallas kernels, shards(): pl.pallas_call(functools.partial(kernel, fs_size, tp_size, halves), out_s...  134 us
    convert_element_type x2, other arithmetic, update(): return (new, moment_new, taken, new.astype(jnp.bfloat16))  7.26 us

commit v1 on v0

v1 whole, which is shorter than its diff:
```python
import functools

import jax
import jax.numpy as jnp
from jax import lax
from jax.experimental import pallas as pl
from jax.experimental.pallas import tpu as pltpu
from jax.sharding import PartitionSpec as P

BETA = 0.9
LEARN_RATE = 0.02
EPSILON = 1e-06
MESH = pl.DeviceIdType.MESH
LANES = 128


def split_dot(value, factor):
    high = value.astype(jnp.bfloat16)
    low = (value - high.astype(jnp.float32)).astype(jnp.bfloat16)
    return jnp.dot(high, factor, preferred_element_type=jnp.float32) + jnp.dot(
        low, factor, preferred_element_type=jnp.float32
    )


def split_dot_left(factor, value):
    high = value.astype(jnp.bfloat16)
    low = (value - high.astype(jnp.float32)).astype(jnp.bfloat16)
    return jnp.dot(factor, high, preferred_element_type=jnp.float32) + jnp.dot(
        factor, low, preferred_element_type=jnp.float32
    )


def token_dot(left, right):
    return lax.dot_general(left, right, (((0,), (0,)), ((), ())), preferred_element_type=jnp.float32)


def folded_squares(value):
    squares = value * value
    rows, width = squares.shape
    total = jnp.sum(squares.reshape(rows // 8, 8, width), axis=0)
    result = total[:, :LANES]
    for start in range(LANES, width, LANES):
        result = result + total[:, start : start + LANES]
    return result


def kernel(
    fs_size, tp_size, halves,
    normed_hbm, rec_cot_hbm, conv_hbm, gate_cot_hbm, rec_moment_hbm, rec_right_hbm, gate_moment_hbm, gate_left_hbm,
    gate_right_hbm,
    rec_new, gate_new, scales,
    normed, rec_cot, conv_out, gate_cot, rec_moment, rec_right, gate_moment, gate_left, gate_right,
    part, first, second, along, helped, grad,
    gate_part, gate_first, gate_second, gate_held, gate_along, gate_grad, gate_pre,
    sums, message, slots,
    in_sem, pair_send, pair_recv, ring_send, ring_recv, help_send, help_recv, cube_send, cube_recv, sum_send, sum_recv,
):
    fs, rep, tp = lax.axis_index("fs"), lax.axis_index("rep"), lax.axis_index("tp")
    bits = (lax.rem(rep, 2), rep // 2)
    partners = (rep + 1 - 2 * bits[0], rep + 2 - 4 * bits[1])
    chunks, rows, width = part.shape[0], part.shape[-2], part.shape[-1]
    half_rows = 8 * rows
    fs_rows = halves * half_rows
    blocks = gate_moment.shape[0]
    masks = [2**i - 1 for i in range(1, fs_size.bit_length())]
    by_head = gate_pre is not None
    last = fs_size - 1
    gate = chunks

    copies = []
    starts = {}

    def load(name, source, target):
        copy = pltpu.make_async_copy(source, target, in_sem.at[len(copies)])
        copies.append(copy)
        starts.setdefault(name, []).append(copy)

    def column(k):
        return slice(k * width, (k + 1) * width)

    def load_half(half):
        for owner in range(fs_size):
            begin = owner * fs_rows + half * half_rows
            span = slice(begin, begin + half_rows)
            load(("normed", half), normed_hbm.at[:, span], normed.at[:, span])

    load(("cot", 0), rec_cot_hbm.at[:, column(0)], rec_cot.at[:, column(0)])
    load_half(0)
    load("gate", conv_hbm, conv_out)
    load("gate", gate_cot_hbm, gate_cot)
    for half in range(1, halves):
        load_half(half)
    for k in range(1, chunks // halves):
        load(("cot", k), rec_cot_hbm.at[:, column(k)], rec_cot.at[:, column(k)])
    load("right", rec_right_hbm, rec_right)
    load("moment", rec_moment_hbm, rec_moment)
    load("factors", gate_right_hbm, gate_right)
    load("factors", gate_left_hbm, gate_left)
    load("gate moment", gate_moment_hbm, gate_moment)
    for copy in copies:
        copy.start()

    def loaded(name):
        for copy in starts.pop(name, ()):
            copy.wait()

    others = [(i, j) for i in range(fs_size) for j in range(tp_size) if i or j]
    direct = len(others) < 16
    if not direct:
        others = [(i, 0) for i in range(1, fs_size)] + [(0, j) for j in range(1, tp_size)]
    peers = [{"fs": lax.rem(fs + i, fs_size), "tp": lax.rem(tp + j, tp_size)} for i, j in others]

    barrier = pltpu.get_barrier_semaphore()
    greeted = peers + [{"rep": p} for p in partners]
    for peer in greeted:
        pl.semaphore_signal(barrier, inc=1, device_id=peer, device_id_type=MESH)
    sums[...] = jnp.zeros_like(sums)

    def remote(source, target, send, recv, peer):
        return pltpu.make_async_remote_copy(
            src_ref=source, dst_ref=target, send_sem=send, recv_sem=recv,
            device_id=peer, device_id_type=MESH,
        )

    def mine(s):
        return bits[s], bits[1 - s]

    def pair(unit, s, index, side, source, target):
        return remote(
            source, target, pair_send.at[unit, s, index], pair_recv.at[unit, s, index], {"rep": partners[side]}
        )

    def first_pair(k, s):
        a, _ = mine(s)
        return pair(k, s, 0, s, part.at[k, s, 1 - a], first.at[k, s])

    def second_pair(k, s):
        a, b = mine(s)
        return pair(k, s, 1, 1 - s, part.at[k, s, a, 1 - b, fs], second.at[k, s])

    def gather_pair(k, s, level):
        a, b = mine(s)
        whole = gate_grad if k == gate else grad.at[k]
        here = whole.at[s, a, b] if level == 0 else whole.at[s, a]
        return pair(k, s, 2 + level, 1 - s if level == 0 else s, here, here)

    def ring(k, s, step):
        a, _ = mine(s)
        peer = lax.rem(fs + step, fs_size)
        return remote(
            part.at[k, s, a, :, peer], along.at[k, s, step - 1],
            ring_send.at[k, s, step - 1], ring_recv.at[k, s, step - 1], {"fs": peer},
        )

    def helper(k, s):
        a, _ = mine(s)
        return remote(
            part.at[k, s, a, :, last - fs], helped.at[k, s], help_send.at[k, s], help_recv.at[k, s],
            {"fs": jnp.where(fs == 0, 1, last - 1)},
        )

    at_end = (fs == 0) | (fs == last)
    beside = (fs == 1) | (fs == last - 1)
    fold_step = jnp.where(fs == 1, last - 1, 2)

    def when(condition, action):
        if condition is None:
            action()
        else:
            pl.when(condition)(action)

    def sends(step):
        skip = []
        if step == last:
            skip.append(fs == 0)
        if step == 1:
            skip.append(fs == last)
        if step == last - 1:
            skip.append(fs == 1)
        if step == 2:
            skip.append(fs == last - 1)
        return jnp.logical_not(functools.reduce(jnp.logical_or, skip)) if skip else None

    def receives(step):
        if step == last:
            return fs != last
        if step == 1:
            return fs != 0
        return None

    def product(unit):
        if unit == gate:
            loaded("gate")

            @pl.loop(0, blocks)
            def _(block):
                columns = pl.ds(pl.multiple_of(block * width, width), width)
                term = token_dot(conv_out[:, columns], gate_cot[:, columns])
                if by_head:
                    each, half = gate_part.shape[3], gate_part.shape[4]
                    head, place = block // each, lax.rem(block, each)
                    gate_part[0, head // 2, lax.rem(head, 2), place] = term[:half]
                    gate_part[1, lax.rem(head, 2), head // 2, place] = term[half:]
                else:
                    gate_part[:, :, :, block] = term.reshape(2, 2, 2, gate_part.shape[4], width)
        else:
            k, half = unit // halves, unit % halves
            loaded(("cot", k))
            loaded(("normed", half))

            @pl.loop(0, fs_size)
            def _(owner):
                start = pl.multiple_of(owner * fs_rows + half * half_rows, half_rows)
                term = token_dot(normed[:, pl.ds(start, half_rows)], rec_cot[:, column(k)])
                part[unit, :, :, :, owner] = term.reshape(2, 2, 2, rows, width)

    def open_rec(k):
        product(k)
        if k == 0:
            pl.semaphore_wait(barrier, len(greeted))
        for s in range(2):
            first_pair(k, s).start()

    def spread(k):
        for s in range(2):
            first_pair(k, s).wait_recv()
            a, _ = mine(s)

            @pl.loop(0, fs_size)
            def _(owner):
                for b in range(2):
                    part[k, s, a, b, owner] += first[k, s, b, owner]

            pl.when(at_end)(lambda s=s: helper(k, s).start())
            for step in range(1, fs_size):
                when(sends(step), lambda s=s, step=step: ring(k, s, step).start())

    def fold(k):
        @pl.when(beside)
        def _():
            for s in range(2):
                helper(k, s).wait_recv()
                a, _ = mine(s)
                part[k, s, a, :, lax.rem(fs + fold_step, fs_size)] += helped[k, s]
                ring(k, s, fold_step).start()

    def collect(k):
        for s in range(2):
            a, _ = mine(s)
            for step in range(1, fs_size):
                def take(s=s, step=step, a=a):
                    ring(k, s, step).wait_recv()
                    part[k, s, a, :, fs] += along[k, s, step - 1]

                when(receives(step), take)
            second_pair(k, s).start()

    def settle(k):
        for s in range(2):
            second_pair(k, s).wait_recv()
            a, b = mine(s)
            grad[k, s, a, b] = part[k, s, a, b, fs] + second[k, s]
            gather_pair(k, s, 0).start()

    def forward(k):
        for s in range(2):
            gather_pair(k, s, 0).wait_recv()
            gather_pair(k, s, 1).start()

    def finish(k):
        for s in range(2):
            gather_pair(k, s, 1).wait_recv()
        loaded("right")
        loaded("moment")
        columns = column(k // halves)
        here = slice(k % halves * half_rows, (k % halves + 1) * half_rows)
        gradient = grad[k].reshape(half_rows, width)
        moment = BETA * rec_moment[here, columns] + split_dot(gradient, rec_right[columns, :])
        rec_new[here, columns] = moment
        sums[0] += folded_squares(gradient)
        sums[1] += folded_squares(moment)

    def gate_pair(s, index):
        a, b = mine(s)
        if index == 0:
            return pair(gate, s, 0, s, gate_part.at[s, 1 - a], gate_first.at[s])
        return pair(gate, s, 1, 1 - s, gate_part.at[s, a, 1 - b], gate_second.at[s])

    def cube(s, step):
        mask = masks[step] if s == 0 else masks[-1 - step]
        return remote(
            gate_held.at[s, step], gate_along.at[s, step], cube_send.at[s, step], cube_recv.at[s, step],
            {"fs": fs ^ mask},
        )

    def pre_pair(level):
        here = gate_pre.at[bits[0], bits[1]] if level == 0 else gate_pre.at[bits[0]]
        return pair(gate, 0, 2 + level, 1 - level, here, here)

    def open_gate():
        product(gate)
        for s in range(2):
            gate_pair(s, 0).start()

    def gate_add_first():
        for s in range(2):
            gate_pair(s, 0).wait_recv()
            a, _ = mine(s)
            gate_part[s, a] += gate_first[s]
            gate_pair(s, 1).start()

    def gate_add_second():
        for s in range(2):
            gate_pair(s, 1).wait_recv()
            a, b = mine(s)
            gate_held[s, 0] = gate_part[s, a, b] + gate_second[s]
            cube(s, 0).start()

    def gate_cube(step):
        for s in range(2):
            cube(s, step).wait_recv()
            total = gate_held[s, step] + gate_along[s, step]
            if step + 1 < len(masks):
                gate_held[s, step + 1] = total
                cube(s, step + 1).start()
            elif by_head:
                half = gate_part.shape[4]
                gate_grad[:, s * half : (s + 1) * half] = total
            else:
                a, b = mine(s)
                gate_grad[s, a, b] = total
                gather_pair(gate, s, 0).start()
        if by_head and step + 1 == len(masks):
            loaded("factors")
            each, own = gate_part.shape[3], gate_left.shape[1]
            for place in range(each):
                block = (2 * bits[0] + bits[1]) * each + place
                gradient = gate_grad[place]
                right_done = split_dot(gradient, gate_right[block])
                gate_pre[bits[0], bits[1], place, 0:own] = split_dot_left(gate_left[block], right_done)
                gate_pre[bits[0], bits[1], place, own:] = jnp.concatenate(
                    [folded_squares(gradient), jnp.zeros((8, width - LANES), jnp.float32)], axis=1
                )
            pre_pair(0).start()

    def gate_forward():
        if by_head:
            pre_pair(0).wait_recv()
            pre_pair(1).start()
        else:
            forward(gate)

    def gate_finish():
        loaded("gate moment")
        if by_head:
            pre_pair(1).wait_recv()
            each, own = gate_part.shape[3], gate_left.shape[1]
            for block in range(blocks):
                head, place = block // each, block % each
                moment = BETA * gate_moment[block] + gate_pre[head // 2, head % 2, place, 0:own]
                gate_new[block] = moment
                sums[2] += gate_pre[head // 2, head % 2, place, own:, 0:LANES] * (1.0 / fs_size)
                sums[3] += folded_squares(moment)
        else:
            for s in range(2):
                gather_pair(gate, s, 1).wait_recv()
            loaded("factors")

            @pl.loop(0, blocks)
            def _(block):
                gradient = gate_grad[:, :, :, block].reshape(width, width)
                right_done = split_dot(gradient, gate_right[block])
                moment = BETA * gate_moment[block] + split_dot_left(gate_left[block], right_done)
                gate_new[block] = moment
                sums[2] += folded_squares(gradient) * (1.0 / fs_size)
                sums[3] += folded_squares(moment)

    def rec_stages(k):
        return [functools.partial(f, k) for f in (open_rec, spread, fold, collect, settle, forward, finish)]

    gate_stages = [open_gate, gate_add_first, gate_add_second]
    gate_stages += [functools.partial(gate_cube, step) for step in range(len(masks))]
    gate_stages += [gate_forward, gate_finish]
    units = [rec_stages(k) for k in range(chunks)]
    units.insert(1, gate_stages)

    for tick in range(len(units) + max(len(unit) for unit in units)):
        for place in range(min(tick, len(units) - 1), -1, -1):
            stage = tick - place
            if stage < len(units[place]):
                units[place][stage]()

    for i in range(4):
        message[i : i + 1] = jnp.sum(sums[i], axis=0, keepdims=True)
    message[4:8] = jnp.zeros((4, LANES), jnp.float32)

    def exchange(begin, end):
        trades = [
            remote(message, slots.at[i], sum_send.at[i], sum_recv.at[i], peers[i]) for i in range(begin, end)
        ]
        for trade in trades:
            trade.start()
        for trade in trades:
            trade.wait()
        total = message[...]
        for i in range(begin, end):
            total = total + slots[i]
        return total

    if direct:
        total = exchange(0, len(peers))
    else:
        message[...] = exchange(0, fs_size - 1)
        total = exchange(fs_size - 1, len(peers))
    squares = [jnp.sum(total[i : i + 1], keepdims=True) for i in range(4)]
    rec_scale = jnp.sqrt(squares[0]) / jnp.sqrt(squares[1] + EPSILON)
    gate_scale = jnp.sqrt(squares[2]) / jnp.sqrt(squares[3] + EPSILON)
    scales[0] = jnp.broadcast_to(rec_scale, (8, LANES))
    scales[1] = jnp.broadcast_to(gate_scale, (8, LANES))

    for s in range(2):
        for k in range(chunks):
            first_pair(k, s).wait_send()
            second_pair(k, s).wait_send()
            pl.when(at_end)(lambda k=k, s=s: helper(k, s).wait_send())
            pl.when(beside)(lambda k=k, s=s: ring(k, s, fold_step).wait_send())
            for step in range(1, fs_size):
                when(sends(step), lambda k=k, s=s, step=step: ring(k, s, step).wait_send())
            for level in range(2):
                gather_pair(k, s, level).wait_send()
        for index in range(2):
            gate_pair(s, index).wait_send()
            if not by_head:
                gather_pair(gate, s, index).wait_send()
        for step in range(len(masks)):
            cube(s, step).wait_send()
    if by_head:
        for level in range(2):
            pre_pair(level).wait_send()


def shards(fs_size, rep_size, tp_size, normed, rec_cot, conv_out, gate_cot, rec_weight, rec_moment,
           rec_right, gate_weight, gate_moment, gate_left, gate_right):
    assert rep_size == 4 and fs_size & (fs_size - 1) == 0 and fs_size >= 4
    f32 = jnp.float32
    fs_rows, columns = rec_weight.shape
    width = rec_right.shape[1]
    blocks, gate_rows = gate_weight.shape[:2]
    halves = 2 if fs_rows % 256 == 0 else 1
    chunks = columns // width * halves
    rows = fs_rows // (8 * halves)
    others = fs_size - 1
    cubes = fs_size.bit_length() - 1
    peers = fs_size * tp_size - 1 if fs_size * tp_size <= 16 else fs_size + tp_size - 2
    loads = columns // width + halves * fs_size + 7
    operands = (normed, rec_cot, conv_out, gate_cot, rec_moment, rec_right, gate_moment, gate_left, gate_right)
    vmem = pl.BlockSpec(memory_space=pltpu.VMEM)
    if blocks % 4 == 0:
        piece = (blocks // 4, width // 2, width)
        gate_grad = pltpu.VMEM((blocks // 4, width, width), f32)
        gate_pre = pltpu.VMEM((2, 2, blocks // 4, gate_rows + 8, width), f32)
    else:
        piece = (blocks, width // 8, width)
        gate_grad = pltpu.VMEM((2, 2, 2, *piece), f32)
        gate_pre = None
    rec_new, gate_new, scales = pl.pallas_call(
        functools.partial(kernel, fs_size, tp_size, halves),
        out_shape=(
            jax.ShapeDtypeStruct(rec_weight.shape, f32),
            jax.ShapeDtypeStruct(gate_weight.shape, f32),
            jax.ShapeDtypeStruct((2, 8, LANES), f32),
        ),
        in_specs=[pl.BlockSpec(memory_space=pltpu.HBM)] * len(operands),
        out_specs=(vmem,) * 3,
        scratch_shapes=[
            *(pltpu.VMEM(x.shape, x.dtype) for x in operands),
            pltpu.VMEM((chunks, 2, 2, 2, fs_size, rows, width), f32),
            pltpu.VMEM((chunks, 2, 2, fs_size, rows, width), f32),
            pltpu.VMEM((chunks, 2, rows, width), f32),
            pltpu.VMEM((chunks, 2, others, 2, rows, width), f32),
            pltpu.VMEM((chunks, 2, 2, rows, width), f32),
            pltpu.VMEM((chunks, 2, 2, 2, rows, width), f32),
            pltpu.VMEM((2, 2, 2, *piece), f32),
            pltpu.VMEM((2, 2, *piece), f32),
            pltpu.VMEM((2, *piece), f32),
            pltpu.VMEM((2, cubes, *piece), f32),
            pltpu.VMEM((2, cubes, *piece), f32),
            gate_grad,
            gate_pre,
            pltpu.VMEM((4, 8, LANES), f32),
            pltpu.VMEM((8, LANES), f32),
            pltpu.VMEM((peers, 8, LANES), f32),
            pltpu.SemaphoreType.DMA((loads,)),
            pltpu.SemaphoreType.DMA((chunks + 1, 2, 4)),
            pltpu.SemaphoreType.DMA((chunks + 1, 2, 4)),
            pltpu.SemaphoreType.DMA((chunks, 2, others)),
            pltpu.SemaphoreType.DMA((chunks, 2, others)),
            pltpu.SemaphoreType.DMA((chunks, 2)),
            pltpu.SemaphoreType.DMA((chunks, 2)),
            pltpu.SemaphoreType.DMA((2, cubes)),
            pltpu.SemaphoreType.DMA((2, cubes)),
            pltpu.SemaphoreType.DMA((peers,)),
            pltpu.SemaphoreType.DMA((peers,)),
        ],
        compiler_params=pltpu.CompilerParams(
            collective_id=0, has_side_effects=True, vmem_limit_bytes=62 * 1024 * 1024
        ),
    )(*operands)

    def update(weight, moment_new, scale):
        taken = LEARN_RATE * scale * moment_new
        new = weight - taken
        return new, moment_new, taken, new.astype(jnp.bfloat16)

    return update(rec_weight, rec_new, scales[0, 0, 0]) + update(gate_weight, gate_new, scales[1, 0, 0])


def solution(mesh):
    in_specs = (
        P(("fs", "rep"), None),
        P(("fs", "rep"), "tp"),
        P(("fs", "rep"), "tp"),
        P(("fs", "rep"), "tp"),
        P("fs", "tp"),
        P("fs", "tp"),
        P("tp", None),
        P("tp", "fs", None),
        P("tp", "fs", None),
        P("tp", "fs", None),
        P("tp", None, None),
    )
    out_specs = (P("fs", "tp"),) * 4 + (P("tp", "fs", None),) * 4
    body = functools.partial(shards, mesh.shape["fs"], mesh.shape["rep"], mesh.shape["tp"])
    return jax.shard_map(body, mesh=mesh, in_specs=in_specs, out_specs=out_specs, check_vma=False)
```

time: 145 us -> 129 us (0.89)
  Pallas kernels: 134 us -> 117 us
  local copies, waits for them, and re-layouts: 1.23 us -> 3.23 us
    pallas_call x1, Pallas kernels: 134 us -> 117 us  [shards(): pl.pallas_call(functools.partial(kernel, fs_size, tp_size, halves), out_s...]
    unnamed x8, local copies, waits for them, and re-layouts: 0.02 us -> 2.04 us
where the time goes in v1:
time: 129 us; the launch traced here: 128 us
  Pallas kernels  117 us (91%)
  other arithmetic  6.52 us (5%)
  local copies, waits for them, and re-layouts  3.23 us (3%)
  between operations  1.99 us (2%)
    pallas_call x1, Pallas kernels, shards(): pl.pallas_call(functools.partial(kernel, fs_size, tp_size, halves), out_s...  117 us
    convert_element_type x2, other arithmetic, update(): return (new, moment_new, taken, new.astype(jnp.bfloat16))  6.52 us

profile of v1, /device:TPU:0, one launch (start us, length us, event | category | flops | bytes accessed | tf_op | source)
XLA Modules:
  0.0 128.4 jit_solution(18262748264941860501)
XLA Ops:
  0.6 116.6 %shard_map.170 = (f32[512,1024]{1,0:T(8,128)}, f32[4,64,256]{2,1,0:T(8,128)}, f32[2,8,128]{2,1,0:T(8,128)}) custom-call(bf16[640,2048]{1,0:T(8,128)(2,1)} %normed_hbm.1, bf16[640,1024]{1,0:T(8,128)(2,1)} %rec_cot_hbm.1, bf16[640,1024]{1,0:T(8,128)(2,1)} %conv_hbm.1, bf16[640,1024]{1,0:T(8,128)(2,1)} %gate_cot_hbm.1, f32[512,1024]{1,0:T(8,128)} %rec_moment_hbm.1, ...), custom_call_target="tpu_custom_call" | custom-call | tf_op jit(solution)/shard_map/pallas_call | solution.py:466
  117.3 1.2 fusion.2
  119.1 0.0 copy-start.1
  119.1 0.0 copy-start.2
  119.1 0.0 copy-start
  119.1 5.6 %fusion.1 = (bf16[512,1024]{1,0:T(8,128)(2,1)}, f32[512,1024]{1,0:T(8,128)}, f32[512,1024]{1,0:T(8,128)}) fusion(f32[512,1024]{1,0:T(8,128)} %param.15, f32[512,1024]{1,0:T(8,128)} %get-tuple-element.31, f32[]{:T(128)} %bitcast), kind=kLoop, calls=%fused_computation.3 | loop fusion | flops 1572864 | bytes 9437188 | tf_op jit(solution)/shard_map/convert_element_type | solution.py:513
  125.4 0.0 copy-done.1
  125.4 0.0 copy-done.2
  125.4 0.9 fusion
  126.3 0.0 copy-done
  126.3 1.3 %copy.21 = f32[512,1024]{1,0:T(8,128)} copy(f32[512,1024]{1,0:T(8,128)S(1)} %copy-done) | data formatting | bytes 4194304
  127.6 0.7 copy.22
Async XLA Ops:
  119.1 6.3 %copy-start.1 = (f32[4,64,256]{2,1,0:T(8,128)S(1)}, f32[4,64,256]{2,1,0:T(8,128)}, u32[]{:S(2)}) copy-start(f32[4,64,256]{2,1,0:T(8,128)} %get-tuple-element.35) | copy-start | bytes 786436
  119.1 6.3 %copy-start.2 = (f32[4,64,256]{2,1,0:T(8,128)S(1)}, f32[4,64,256]{2,1,0:T(8,128)}, u32[]{:S(2)}) copy-start(f32[4,64,256]{2,1,0:T(8,128)} %param.18) | copy-start | bytes 786436
  119.1 7.2 %copy-start = (f32[512,1024]{1,0:T(8,128)S(1)}, f32[512,1024]{1,0:T(8,128)}, u32[]{:S(2)}) copy-start(f32[512,1024]{1,0:T(8,128)} %get-tuple-element.31) | copy-start | bytes 6291460

commit v2 on v1

v2 whole, which is shorter than its diff:
```python
import functools
import itertools
import math

import jax
import jax.numpy as jnp
from jax import lax
from jax.experimental import pallas as pl
from jax.experimental.pallas import tpu as pltpu
from jax.sharding import PartitionSpec as P

BETA = 0.9
LEARN_RATE = 0.02
EPSILON = 1e-06
MESH = pl.DeviceIdType.MESH
LANES = 128
PARTS = 4
GATE_PLACE = 7
REC_AT = (0, 1, 2, 3, 4, 5, 6)
GATE_AT = (0, 1, 2, 3, 4, 5, 6, 7)


def split_dot(value, factor):
    high = value.astype(jnp.bfloat16)
    low = (value - high.astype(jnp.float32)).astype(jnp.bfloat16)
    return jnp.dot(high, factor, preferred_element_type=jnp.float32) + jnp.dot(
        low, factor, preferred_element_type=jnp.float32
    )


def split_dot_left(factor, value):
    high = value.astype(jnp.bfloat16)
    low = (value - high.astype(jnp.float32)).astype(jnp.bfloat16)
    return jnp.dot(factor, high, preferred_element_type=jnp.float32) + jnp.dot(
        factor, low, preferred_element_type=jnp.float32
    )


def token_dot(left, right):
    return lax.dot_general(left, right, (((0,), (0,)), ((), ())), preferred_element_type=jnp.float32)


def folded_squares(value):
    squares = value * value
    rows, width = squares.shape
    total = jnp.sum(squares.reshape(rows // 8, 8, width), axis=0)
    result = total[:, :LANES]
    for start in range(LANES, width, LANES):
        result = result + total[:, start : start + LANES]
    return result


def plan(fs_rows, column_count):
    units = []
    for column in range(column_count):
        sizes = [256] * (fs_rows // 256) or [fs_rows]
        if len(sizes) > 1 and column == 0:
            sizes = [128, 128] + sizes[1:]
        if len(sizes) > 1 and column == column_count - 1:
            sizes = sizes[:-1] + [128, 128]
        start = 0
        for size in sizes:
            units.append((column, start, size, (column * fs_rows + start) // 8))
            start += size
    return units


def kernel(
    fs_size, tp_size, units,
    normed_hbm, rec_cot_hbm, conv_hbm, gate_cot_hbm, rec_moment_hbm, rec_right_hbm, gate_moment_hbm, gate_left_hbm,
    gate_right_hbm,
    rec_new, gate_new, scales,
    normed, rec_cot, conv_out, gate_cot, rec_moment, rec_right, gate_moment, gate_left, gate_right,
    part, first, second, along, helped, grad,
    gate_part, gate_first, gate_second, gate_held, gate_along, gate_helped, gate_grad, gate_pre,
    sums, message, slots,
    in_sem, rec_send, pair_recv, ring_recv, help_recv,
    gate_send, gate_recv, spread_recv, pre_send, pre_recv, cube_send, cube_recv, sum_send, sum_recv,
):
    fs, rep, tp = lax.axis_index("fs"), lax.axis_index("rep"), lax.axis_index("tp")
    bits = (lax.rem(rep, 2), rep // 2)
    partners = (rep + 1 - 2 * bits[0], rep + 2 - 4 * bits[1])
    width = part.shape[-1]
    fs_rows = rec_moment.shape[0]
    blocks = gate_moment.shape[0]
    masks = [2**i - 1 for i in range(1, fs_size.bit_length())]
    by_head = gate_pre is not None
    last = fs_size - 1
    gate = len(units)

    copies = []
    waits = {}

    def load(name, source, target, sem=None):
        sem = in_sem.at[len(waits)] if sem is None else sem
        copies.append(pltpu.make_async_copy(source, target, sem))
        waits.setdefault(name, (target, sem))
        return sem

    def column_of(k):
        return slice(units[k][0] * width, (units[k][0] + 1) * width)

    def fetch_columns(column):
        span = slice(column * width, (column + 1) * width)
        load(("cot", column), rec_cot_hbm.at[:, span], rec_cot.at[:, span])

    fetch_columns(0)
    for column, start, size, _ in units:
        if column == 0:
            sem = None
            for owner in range(fs_size):
                span = slice(owner * fs_rows + start, owner * fs_rows + start + size)
                sem = load(("normed", start), normed_hbm.at[:, span], normed.at[:, span], sem)
            waits["normed", start] = (normed.at[:, 0 : fs_size * size], sem)
            if start == 0:
                load("conv", conv_hbm, conv_out)
                load("gate", gate_cot_hbm, gate_cot)
    for column in range(1, units[-1][0] + 1):
        fetch_columns(column)
    load("right", rec_right_hbm, rec_right)
    load("moment", rec_moment_hbm, rec_moment)
    load("gate right", gate_right_hbm, gate_right)
    load("gate left", gate_left_hbm, gate_left)
    load("gate moment", gate_moment_hbm, gate_moment)
    for copy in copies:
        copy.start()

    def loaded(*names):
        for name in names:
            if name in waits:
                whole, sem = waits.pop(name)
                pltpu.make_async_copy(whole, whole, sem).wait()

    sizes = {"fs": fs_size, "rep": 4, "tp": tp_size}
    places = {"fs": fs, "rep": rep, "tp": tp}
    direct = math.prod(sizes.values()) <= 32
    groups = [tuple(sizes)] if direct else [(axis,) for axis in ("rep", "fs", "tp")]
    counts = [math.prod(sizes[axis] for axis in axes) for axes in groups]

    def members(axes):
        return [
            {axis: lax.rem(places[axis] + move, sizes[axis]) for axis, move in zip(axes, moves)}
            for moves in itertools.product(*(range(sizes[axis]) for axis in axes))
            if any(moves)
        ]

    barrier = pltpu.get_barrier_semaphore()
    greeted = [peer for axes in groups for peer in members(axes)]
    for peer in greeted:
        pl.semaphore_signal(barrier, inc=1, device_id=peer, device_id_type=MESH)
    sums[...] = jnp.zeros_like(sums)

    def remote(source, target, send, recv, peer):
        return pltpu.make_async_remote_copy(
            src_ref=source, dst_ref=target, send_sem=send, recv_sem=recv,
            device_id=peer, device_id_type=MESH,
        )

    def arrived(whole, recv):
        remote(whole, whole, rec_send.at[0], recv, {"rep": partners[0]}).wait_recv()

    def sent(whole, send):
        remote(whole, whole, send, pair_recv.at[0, 0], {"rep": partners[0]}).wait_send()

    def mine(s):
        return bits[s], bits[1 - s]

    def rows_of(k):
        return slice(units[k][3], units[k][3] + units[k][2] // 8)

    def first_pair(k, s):
        a, _ = mine(s)
        here = rows_of(k)
        return remote(
            part.at[s, 1 - a, :, :, here], first.at[s, :, :, here], rec_send.at[0], pair_recv.at[k, 0],
            {"rep": partners[s]},
        )

    def second_pair(k, s):
        a, b = mine(s)
        here = rows_of(k)
        return remote(
            part.at[s, a, 1 - b, fs, here], second.at[s, here], rec_send.at[2], pair_recv.at[k, 1],
            {"rep": partners[1 - s]},
        )

    def gather_pair(k, s, level):
        a, b = mine(s)
        if level == 0:
            here = grad.at[s, a, b, rows_of(k)]
        else:
            here = grad.at[s, a, :, rows_of(k)]
        return remote(
            here, here, rec_send.at[2], pair_recv.at[k, 2 + level], {"rep": partners[1 - s if level == 0 else s]}
        )

    def chunk(k, s, owner):
        a, b = mine(s)
        return gate_part.at[s, a, b, owner] if k == gate else part.at[s, a, :, owner, rows_of(k)]

    def ring_slot(k, s, step):
        return gate_along.at[s, step - 1] if k == gate else along.at[s, step - 1, :, rows_of(k)]

    def help_slot(k, s):
        return gate_helped.at[s] if k == gate else helped.at[s, :, rows_of(k)]

    def ring_sem(k):
        return gate_send.at[2] if k == gate else rec_send.at[1]

    def ring(k, s, step):
        peer = lax.rem(fs + step, fs_size)
        return remote(chunk(k, s, peer), ring_slot(k, s, step), ring_sem(k), ring_recv.at[k], {"fs": peer})

    def helper(k, s):
        return remote(
            chunk(k, s, last - fs), help_slot(k, s), ring_sem(k), help_recv.at[k],
            {"fs": jnp.where(fs == 0, 1, last - 1)},
        )

    at_end = (fs == 0) | (fs == last)
    beside = (fs == 1) | (fs == last - 1)
    fold_step = jnp.where(fs == 1, last - 1, 2)

    def when(condition, action):
        if condition is None:
            action()
        else:
            pl.when(condition)(action)

    def sends(step):
        skip = []
        if step == last:
            skip.append(fs == 0)
        if step == 1:
            skip.append(fs == last)
        if step == last - 1:
            skip.append(fs == 1)
        if step == 2:
            skip.append(fs == last - 1)
        return jnp.logical_not(functools.reduce(jnp.logical_or, skip)) if skip else None

    def receives(step):
        if step == last:
            return fs != last
        if step == 1:
            return fs != 0
        return None

    def ring_open(k, s):
        pl.when(at_end)(lambda: helper(k, s).start())
        for step in range(1, fs_size):
            when(sends(step), lambda step=step: ring(k, s, step).start())

    def fold(k):
        @pl.when(beside)
        def _():
            arrived(gate_helped if k == gate else helped.at[:, :, rows_of(k)], help_recv.at[k])
            for s in range(2):
                whole = chunk(k, s, lax.rem(fs + fold_step, fs_size))
                whole[...] += help_slot(k, s)[...]
                ring(k, s, fold_step).start()

    def ring_close(k):
        def slots_of(count):
            return gate_along.at[:, 0:count] if k == gate else along.at[:, 0:count, :, rows_of(k)]

        pl.when(at_end)(lambda: arrived(slots_of(last - 1), ring_recv.at[k]))
        pl.when(jnp.logical_not(at_end))(lambda: arrived(slots_of(last), ring_recv.at[k]))
        for s in range(2):
            own = chunk(k, s, fs)
            for step in range(1, fs_size):
                def take(own=own, s=s, step=step):
                    own[...] += ring_slot(k, s, step)[...]

                when(receives(step), take)

    def product(k):
        column, start, size, _ = units[k]
        loaded(("cot", column))
        loaded(("normed", start))

        @pl.loop(0, fs_size)
        def _(owner):
            begin = pl.multiple_of(owner * fs_rows + start, 128)
            term = token_dot(normed[:, pl.ds(begin, size)], rec_cot[:, column_of(k)])
            part[:, :, :, owner, rows_of(k)] = term.reshape(2, 2, 2, size // 8, width)

    def open_rec(k):
        product(k)
        if k == 0:
            pl.semaphore_wait(barrier, len(greeted))
        for s in range(2):
            first_pair(k, s).start()

    def spread(k):
        arrived(first.at[:, :, :, rows_of(k)], pair_recv.at[k, 0])
        for s in range(2):
            a, _ = mine(s)

            @pl.loop(0, fs_size)
            def _(owner):
                for b in range(2):
                    part[s, a, b, owner, rows_of(k)] += first[s, b, owner, rows_of(k)]

            ring_open(k, s)

    def collect(k):
        ring_close(k)
        for s in range(2):
            second_pair(k, s).start()

    def settle(k):
        loaded("right", "moment")
        arrived(second.at[:, rows_of(k)], pair_recv.at[k, 1])
        _, start, size, _ = units[k]
        rows = size // 8
        gradients, moments = [], []
        for s in range(2):
            a, b = mine(s)
            gradients.append(part[s, a, b, fs, rows_of(k)] + second[s, rows_of(k)])
            begin = pl.multiple_of(start + (4 * s + 2 * a + b) * rows, 8)
            moments.append(rec_moment[pl.ds(begin, rows), column_of(k)])
        gradient = jnp.concatenate(gradients, axis=0)
        moment = BETA * jnp.concatenate(moments, axis=0) + split_dot(gradient, rec_right[column_of(k), :])
        for s in range(2):
            a, b = mine(s)
            grad[s, a, b, rows_of(k)] = moment[s * rows : (s + 1) * rows]
            gather_pair(k, s, 0).start()
        sums[0] += folded_squares(gradient)
        sums[1] += folded_squares(moment)

    def forward(k):
        arrived(grad.at[0, :, 0, rows_of(k)], pair_recv.at[k, 2])
        for s in range(2):
            gather_pair(k, s, 1).start()

    def finish(k):
        arrived(grad.at[0, :, :, rows_of(k)], pair_recv.at[k, 3])
        _, start, size, _ = units[k]
        rec_new[start : start + size, column_of(k)] = grad[:, :, :, rows_of(k)].reshape(size, width)

    def gate_pair(s, index):
        a, b = mine(s)
        source, target = (gate_part.at[s, 1 - a], gate_first) if index == 0 else (gate_part.at[s, a, 1 - b], gate_second)
        return remote(
            source, target.at[s], gate_send.at[index], gate_recv.at[index],
            {"rep": partners[s if index == 0 else 1 - s]},
        )

    def open_gate():
        loaded("conv", "gate")

        @pl.loop(0, blocks)
        def _(block):
            columns = pl.ds(pl.multiple_of(block * width, width), width)
            term = token_dot(conv_out[:, columns], gate_cot[:, columns])
            if by_head:
                each, thin = gate_part.shape[4], gate_part.shape[5]
                head, place = block // each, lax.rem(block, each)
                halves = term.reshape(2, fs_size, thin, width)
                gate_part[0, head // 2, lax.rem(head, 2), :, place] = halves[0]
                gate_part[1, lax.rem(head, 2), head // 2, :, place] = halves[1]
            else:
                gate_part[:, :, :, block] = term.reshape(2, 2, 2, gate_part.shape[4], width)

        for s in range(2):
            gate_pair(s, 0).start()

    def gate_add_first():
        arrived(gate_first, gate_recv.at[0])
        for s in range(2):
            a, _ = mine(s)
            gate_part[s, a] += gate_first[s]
            gate_pair(s, 1).start()

    def gate_total(s):
        if s == 0:
            arrived(gate_second, gate_recv.at[1])
        a, b = mine(s)
        return gate_part[s, a, b] + gate_second[s]

    def gate_scatter():
        for s in range(2):
            a, b = mine(s)
            gate_part[s, a, b] = gate_total(s)
            ring_open(gate, s)

    def broadcast(s, step):
        return remote(
            gate_grad.at[s, fs], gate_grad.at[s, fs], gate_send.at[3], spread_recv.at[0],
            {"fs": lax.rem(fs + step, fs_size)},
        )

    def gate_collect():
        ring_close(gate)
        for s in range(2):
            a, b = mine(s)
            gate_grad[s, fs] = gate_part[s, a, b, fs]
            for step in range(1, fs_size):
                broadcast(s, step).start()

    def pre_pair(level):
        here = gate_pre.at[bits[0], bits[1]] if level == 0 else gate_pre.at[bits[0]]
        return remote(here, here, pre_send.at[level], pre_recv.at[level], {"rep": partners[1 - level]})

    def gate_product():
        arrived(gate_along, spread_recv.at[0])
        loaded("gate right", "gate left", "gate moment")
        each = gate_part.shape[4]
        for place in range(each):
            block = (2 * bits[0] + bits[1]) * each + place
            gradient = gate_grad[:, :, place].reshape(width, width)
            right_done = split_dot(gradient, gate_right[block])
            moment = BETA * gate_moment[block] + split_dot_left(gate_left[block], right_done)
            gate_pre[bits[0], bits[1], place] = moment
            sums[2] += folded_squares(gradient) * (1.0 / fs_size)
            sums[3] += folded_squares(moment)
        pre_pair(0).start()

    def gate_forward():
        pre_pair(0).wait_recv()
        pre_pair(1).start()

    def gate_finish():
        pre_pair(1).wait_recv()
        each = gate_part.shape[4]
        for block in range(blocks):
            head, place = block // each, block % each
            gate_new[block] = gate_pre[head // 2, head % 2, place]

    def cube(s, step):
        mask = masks[step] if s == 0 else masks[-1 - step]
        return remote(
            gate_held.at[s, step], gate_along.at[s, step], cube_send.at[s, step], cube_recv.at[s, step],
            {"fs": fs ^ mask},
        )

    def whole_pair(s, level):
        a, b = mine(s)
        here = gate_grad.at[s, a, b] if level == 0 else gate_grad.at[s, a]
        return remote(
            here, here, pre_send.at[2 * s + level], pre_recv.at[2 * s + level],
            {"rep": partners[1 - s if level == 0 else s]},
        )

    def cube_open():
        for s in range(2):
            gate_held[s, 0] = gate_total(s)
            cube(s, 0).start()

    def cube_add(step):
        for s in range(2):
            cube(s, step).wait_recv()
            total = gate_held[s, step] + gate_along[s, step]
            if step + 1 < len(masks):
                gate_held[s, step + 1] = total
                cube(s, step + 1).start()
            else:
                a, b = mine(s)
                gate_grad[s, a, b] = total
                whole_pair(s, 0).start()

    def whole_forward():
        for s in range(2):
            whole_pair(s, 0).wait_recv()
            whole_pair(s, 1).start()

    def whole_finish():
        for s in range(2):
            whole_pair(s, 1).wait_recv()
        loaded("gate right", "gate left", "gate moment")

        @pl.loop(0, blocks)
        def _(block):
            gradient = gate_grad[:, :, :, block].reshape(width, width)
            right_done = split_dot(gradient, gate_right[block])
            moment = BETA * gate_moment[block] + split_dot_left(gate_left[block], right_done)
            gate_new[block] = moment
            sums[2] += folded_squares(gradient) * (0.25 / fs_size)
            sums[3] += folded_squares(moment) * 0.25

    def rec_stages(k):
        return [functools.partial(f, k) for f in (open_rec, spread, fold, collect, settle, forward, finish)]

    gate_stages = [open_gate, gate_add_first]
    if by_head:
        gate_stages += [gate_scatter, functools.partial(fold, gate), gate_collect, gate_product, gate_forward, gate_finish]
    else:
        gate_stages += [cube_open, *(functools.partial(cube_add, step) for step in range(len(masks)))]
        gate_stages += [whole_forward, whole_finish]
    queue = [rec_stages(k) for k in range(len(units))]
    queue.insert(min(GATE_PLACE, len(queue)), gate_stages)

    agenda = []
    for place, stages in enumerate(queue):
        offsets = GATE_AT if stages is gate_stages else REC_AT
        for stage, action in enumerate(stages):
            offset = offsets[stage] if stage < len(offsets) else offsets[-1] + stage + 1 - len(offsets)
            agenda.append((max(0, place + offset), stage > 0, -place if stage else place, stage, action))

    def exchange_open(index):
        axes, base = groups[index], sum(counts[:index])
        me = base
        scale = 1
        for axis in reversed(axes):
            me = me + places[axis] * scale
            scale *= sizes[axis]
        slots[me] = message[...]
        for peer in members(axes):
            remote(message, slots.at[me], sum_send.at[index], sum_recv.at[index], peer).start()

    def exchange_close(index):
        base = sum(counts[:index])
        others = slots.at[base : base + counts[index] - 1]
        arrived(others, sum_recv.at[index])
        sent(others, sum_send.at[index])
        message[...] = jnp.sum(slots[base : base + counts[index]], axis=0)

    adding = {settle, gate_product, whole_finish}
    left = sum(getattr(entry[-1], "func", entry[-1]) in adding for entry in agenda)
    for tick, _, place, stage, action in sorted(agenda, key=lambda entry: entry[:4]):
        action()
        if getattr(action, "func", action) in adding:
            left -= 1
            if not left:
                for i in range(4):
                    message[i : i + 1] = jnp.sum(sums[i], axis=0, keepdims=True)
                message[4:8] = jnp.zeros((4, LANES), jnp.float32)
                exchange_open(0)

    exchange_close(0)
    for index in range(1, len(groups)):
        exchange_open(index)
        exchange_close(index)
    total = message[...]
    squares = [jnp.sum(total[i : i + 1], keepdims=True) for i in range(4)]
    rec_scale = jnp.sqrt(squares[0]) / jnp.sqrt(squares[1] + EPSILON)
    gate_scale = jnp.sqrt(squares[2]) / jnp.sqrt(squares[3] + EPSILON)
    scales[0] = jnp.broadcast_to(rec_scale, (8, LANES))
    scales[1] = jnp.broadcast_to(gate_scale, (8, LANES))

    sent(first, rec_send.at[0])
    sent(along, rec_send.at[1])
    sent(grad, rec_send.at[2])
    sent(gate_first, gate_send.at[0])
    sent(gate_second, gate_send.at[1])
    if by_head:
        sent(gate_along, gate_send.at[2])
        sent(gate_along, gate_send.at[3])
        for level in range(2):
            pre_pair(level).wait_send()
    else:
        for s in range(2):
            for step in range(len(masks)):
                cube(s, step).wait_send()
            for level in range(2):
                whole_pair(s, level).wait_send()


def update_kernel(
    rec_weight, gate_weight, rec_new, gate_new, scales,
    rec_weight_out, rec_new_out, rec_step_out, rec_copy_out,
    gate_weight_out, gate_new_out, gate_step_out, gate_copy_out,
    rec_after, rec_step, rec_copy, gate_after, gate_step, gate_copy,
    out_sem,
):
    groups = (
        (rec_weight, rec_new, rec_after, rec_step, rec_copy, rec_weight_out, rec_new_out, rec_step_out, rec_copy_out),
        (gate_weight, gate_new, gate_after, gate_step, gate_copy,
         gate_weight_out, gate_new_out, gate_step_out, gate_copy_out),
    )
    copies = []
    for group, (weight, new, after, step, copy, *outs) in enumerate(groups):
        parts = PARTS if weight.shape[0] % PARTS == 0 else 1
        size = weight.shape[0] // parts
        factor = LEARN_RATE * scales[group, 0:1, 0:1]
        for i in range(parts):
            here = slice(i * size, (i + 1) * size)
            moved = pltpu.make_async_copy(new.at[here], outs[1].at[here], out_sem.at[group, i, 1])
            moved.start()
            copies.append(moved)
        for i in range(parts):
            here = slice(i * size, (i + 1) * size)
            moment = new[here]
            taken = (factor if moment.ndim == 2 else factor[None]) * moment
            step[here] = taken
            result = weight[here] - taken
            after[here] = result
            copy[here] = result.astype(jnp.bfloat16)
            for index, source in ((0, after), (2, step), (3, copy)):
                moved = pltpu.make_async_copy(source.at[here], outs[index].at[here], out_sem.at[group, i, index])
                moved.start()
                copies.append(moved)
    for moved in copies:
        moved.wait()


def shards(fs_size, rep_size, tp_size, normed, rec_cot, conv_out, gate_cot, rec_weight, rec_moment,
           rec_right, gate_weight, gate_moment, gate_left, gate_right):
    assert rep_size == 4 and fs_size & (fs_size - 1) == 0 and fs_size >= 4
    f32 = jnp.float32
    fs_rows, columns = rec_weight.shape
    width = rec_right.shape[1]
    blocks, gate_rows = gate_weight.shape[:2]
    units = plan(fs_rows, columns // width)
    rows = fs_rows * (columns // width) // 8
    others = fs_size - 1
    cubes = fs_size.bit_length() - 1
    direct = fs_size * rep_size * tp_size <= 32
    groups, tiles = (1, fs_size * rep_size * tp_size) if direct else (3, fs_size + rep_size + tp_size)
    loads = columns // width + sum(unit[0] == 0 for unit in units) + 7
    operands = (normed, rec_cot, conv_out, gate_cot, rec_moment, rec_right, gate_moment, gate_left, gate_right)
    vmem = pl.BlockSpec(memory_space=pltpu.VMEM)
    dma = pltpu.SemaphoreType.DMA
    by_head = blocks % 4 == 0
    if by_head:
        thin = (blocks // 4, width // 2 // fs_size, width)
        piece = (fs_size, *thin)
        gate_held = None
        gate_along = pltpu.VMEM((2, others, *thin), f32)
        gate_helped = pltpu.VMEM((2, *thin), f32)
        gate_grad = pltpu.VMEM((2, *piece), f32)
        gate_pre = pltpu.VMEM((2, 2, blocks // 4, gate_rows, width), f32)
    else:
        piece = (blocks, width // 8, width)
        gate_held = pltpu.VMEM((2, cubes, *piece), f32)
        gate_along = pltpu.VMEM((2, cubes, *piece), f32)
        gate_helped = None
        gate_grad = pltpu.VMEM((2, 2, 2, *piece), f32)
        gate_pre = None
    rec_new, gate_new, scales = pl.pallas_call(
        functools.partial(kernel, fs_size, tp_size, units),
        out_shape=(
            pltpu.VMEM(rec_weight.shape, f32),
            pltpu.VMEM(gate_weight.shape, f32),
            pltpu.VMEM((2, 8, LANES), f32),
        ),
        in_specs=[pl.BlockSpec(memory_space=pltpu.HBM)] * len(operands),
        out_specs=(vmem,) * 3,
        scratch_shapes=[
            *(pltpu.VMEM(x.shape, x.dtype) for x in operands),
            pltpu.VMEM((2, 2, 2, fs_size, rows, width), f32),
            pltpu.VMEM((2, 2, fs_size, rows, width), f32),
            pltpu.VMEM((2, rows, width), f32),
            pltpu.VMEM((2, others, 2, rows, width), f32),
            pltpu.VMEM((2, 2, rows, width), f32),
            pltpu.VMEM((2, 2, 2, rows, width), f32),
            pltpu.VMEM((2, 2, 2, *piece), f32),
            pltpu.VMEM((2, 2, *piece), f32),
            pltpu.VMEM((2, *piece), f32),
            gate_held,
            gate_along,
            gate_helped,
            gate_grad,
            gate_pre,
            pltpu.VMEM((4, 8, LANES), f32),
            pltpu.VMEM((8, LANES), f32),
            pltpu.VMEM((tiles, 8, LANES), f32),
            dma((loads,)),
            dma((3,)),
            dma((len(units), 4)),
            dma((len(units) + 1,)),
            dma((len(units) + 1,)),
            dma((4,)),
            dma((2,)),
            dma((1,)),
            dma((4,)),
            dma((4,)),
            None if by_head else dma((2, cubes)),
            None if by_head else dma((2, cubes)),
            dma((groups,)),
            dma((groups,)),
        ],
        compiler_params=pltpu.CompilerParams(
            collective_id=0, has_side_effects=True, vmem_limit_bytes=44 * 1024 * 1024
        ),
    )(*(pltpu.with_memory_space_constraint(x, pltpu.HBM) for x in operands))

    return update(rec_weight, gate_weight, rec_new, gate_new, scales)


def update(rec_weight, gate_weight, rec_new, gate_new, scales):
    vmem = pl.BlockSpec(memory_space=pltpu.VMEM)
    hbm = pl.BlockSpec(memory_space=pltpu.HBM)
    f32, bf16 = jnp.float32, jnp.bfloat16
    weights = (rec_weight, gate_weight)
    shapes = [jax.ShapeDtypeStruct(w.shape, t) for w in weights for t in (f32, f32, f32, bf16)]
    return pl.pallas_call(
        update_kernel,
        out_shape=shapes,
        in_specs=[vmem] * 5,
        out_specs=[hbm] * 8,
        scratch_shapes=[
            *(pltpu.VMEM(w.shape, t) for w in weights for t in (f32, f32, bf16)),
            pltpu.SemaphoreType.DMA((2, PARTS, 4)),
        ],
        compiler_params=pltpu.CompilerParams(vmem_limit_bytes=16 * 1024 * 1024),
    )(
        *(pltpu.with_memory_space_constraint(x, pltpu.VMEM) for x in (rec_weight, gate_weight, rec_new, gate_new, scales))
    )


def solution(mesh):
    in_specs = (
        P(("fs", "rep"), None),
        P(("fs", "rep"), "tp"),
        P(("fs", "rep"), "tp"),
        P(("fs", "rep"), "tp"),
        P("fs", "tp"),
        P("fs", "tp"),
        P("tp", None),
        P("tp", "fs", None),
        P("tp", "fs", None),
        P("tp", "fs", None),
        P("tp", None, None),
    )
    out_specs = (P("fs", "tp"),) * 4 + (P("tp", "fs", None),) * 4
    body = functools.partial(shards, mesh.shape["fs"], mesh.shape["rep"], mesh.shape["tp"])
    return jax.shard_map(body, mesh=mesh, in_specs=in_specs, out_specs=out_specs, check_vma=False)
```

time: 129 us -> 109 us (0.84)
  Pallas kernels: 117 us -> 108 us
  other arithmetic: 6.52 us -> 0 us
  local copies, waits for them, and re-layouts: 3.23 us -> 0.01 us
  between operations: 1.99 us -> 0.68 us
    pallas_call x1 -> x2, Pallas kernels: 117 us -> 108 us  [the longest x1 104 us: shards(): pl.pallas_call(functools.partial(kernel, fs_size, tp_size, units), out_sh...]
    convert_element_type x2 -> x0, other arithmetic: 6.52 us -> none  [update(): return (new, moment_new, taken, new.astype(jnp.bfloat16))]
    unnamed x8 -> x4, local copies, waits for them, and re-layouts: 2.04 us -> 0.01 us
where the time goes in v2:
time: 109 us; the launch traced here: 108 us
  Pallas kernels  108 us (99%)
    pallas_call x1, Pallas kernels, shards(): pl.pallas_call(functools.partial(kernel, fs_size, tp_size, units), out_sh...  104 us
    pallas_call x1, Pallas kernels, update(): pl.pallas_call(update_kernel, out_shape=shapes, in_specs=[vmem] * 5, out_...  3.5 us

profile of v2, /device:TPU:0, one launch (start us, length us, event | category | flops | bytes accessed | tf_op | source)
XLA Modules:
  0.0 108.4 jit_solution(9468979729507095100)
XLA Ops:
  0.6 0.0 copy-start.1
  0.6 0.0 copy-start
  0.7 104.2 %shard_map.170 = (f32[512,1024]{1,0:T(8,128)S(1)}, f32[4,64,256]{2,1,0:T(8,128)S(1)}, f32[2,8,128]{2,1,0:T(8,128)S(1)}) custom-call(bf16[640,2048]{1,0:T(8,128)(2,1)} %normed_hbm.1, bf16[640,1024]{1,0:T(8,128)(2,1)} %rec_cot_hbm.1, bf16[640,1024]{1,0:T(8,128)(2,1)} %conv_hbm.1, bf16[640,1024]{1,0:T(8,128)(2,1)} %gate_cot_hbm.1, f32[512,1024]{1,0:T(8,128)} %rec_moment_hbm.1, ...), custom_call_target="tpu_custom_call" | custom-call | tf_op jit(solution)/shard_map/pallas_call | solution.py:631
  104.8 0.0 copy-done.1
  104.9 0.0 copy-done
  104.9 3.5 %shard_map.171 = (f32[512,1024]{1,0:T(8,128)}, f32[512,1024]{1,0:T(8,128)}, f32[512,1024]{1,0:T(8,128)}, bf16[512,1024]{1,0:T(8,128)(2,1)}, f32[4,64,256]{2,1,0:...) custom-call(f32[512,1024]{1,0:T(8,128)S(1)} %copy-done, ...), custom_call_target="tpu_custom_call" | custom-call | tf_op jit(solution)/shard_map/pallas_call | solution.py:688
Async XLA Ops:
  0.6 104.2 %copy-start.1 = (f32[4,64,256]{2,1,0:T(8,128)S(1)}, f32[4,64,256]{2,1,0:T(8,128)}, u32[]{:S(2)}) copy-start(f32[4,64,256]{2,1,0:T(8,128)} %gate_weight.1) | copy-start | bytes 786436
  0.6 104.2 %copy-start = (f32[512,1024]{1,0:T(8,128)S(1)}, f32[512,1024]{1,0:T(8,128)}, u32[]{:S(2)}) copy-start(f32[512,1024]{1,0:T(8,128)} %rec_weight.1) | copy-start | bytes 6291460

commit v3 on v2

--- a/solution.py
+++ b/solution.py
@@ -15,9 +15,13 @@
 MESH = pl.DeviceIdType.MESH
 LANES = 128
 PARTS = 4
-GATE_PLACE = 7
+LATE, MIDDLE, FINAL = range(3)
+ALONG_FIRST = 0
+ALONG_LAST = 3
+GATE_PLACE = 5
+OPEN_AT = (0, 0, 1, 2, 4)
 REC_AT = (0, 1, 2, 3, 4, 5, 6)
-GATE_AT = (0, 1, 2, 3, 4, 5, 6, 7)
+GATE_AT = (0, 1, 2, 3, 4, 6, 8, 10)
 
 
 def split_dot(value, factor):
@@ -62,19 +66,28 @@
         for size in sizes:
             units.append((column, start, size, (column * fs_rows + start) // 8))
             start += size
-    return units
+    if len(units) > 4:
+        kinds = [LATE] * ALONG_FIRST + [MIDDLE] * (len(units) - ALONG_FIRST - ALONG_LAST) + [FINAL] * ALONG_LAST
+    else:
+        kinds = [MIDDLE] * len(units)
+    return units, kinds
+
+
+def span_of(units, kinds, wanted):
+    chosen = [unit for unit, kind in zip(units, kinds) if kind in wanted]
+    return slice(chosen[0][3], chosen[-1][3] + chosen[-1][2] // 8) if chosen else None
 
 
 def kernel(
-    fs_size, tp_size, units,
+    fs_size, tp_size, units, kinds,
     normed_hbm, rec_cot_hbm, conv_hbm, gate_cot_hbm, rec_moment_hbm, rec_right_hbm, gate_moment_hbm, gate_left_hbm,
     gate_right_hbm,
     rec_new, gate_new, scales,
     normed, rec_cot, conv_out, gate_cot, rec_moment, rec_right, gate_moment, gate_left, gate_right,
-    part, first, second, along, helped, grad,
+    part, first, second, along, helped, grad, wide_along, wide_helped, thick_second,
     gate_part, gate_first, gate_second, gate_held, gate_along, gate_helped, gate_grad, gate_pre,
     sums, message, slots,
-    in_sem, rec_send, pair_recv, ring_recv, help_recv,
+    in_sem, rec_send, kind_send, pair_recv, ring_recv, help_recv,
     gate_send, gate_recv, spread_recv, pre_send, pre_recv, cube_send, cube_recv, sum_send, sum_recv,
 ):
     fs, rep, tp = lax.axis_index("fs"), lax.axis_index("rep"), lax.axis_index("tp")
@@ -133,8 +146,8 @@
 
     sizes = {"fs": fs_size, "rep": 4, "tp": tp_size}
     places = {"fs": fs, "rep": rep, "tp": tp}
-    direct = math.prod(sizes.values()) <= 32
-    groups = [tuple(sizes)] if direct else [(axis,) for axis in ("rep", "fs", "tp")]
+    direct = fs_size * tp_size <= 8
+    groups = [("fs", "tp"), ("rep",)] if direct else [("fs",), ("tp",), ("rep",)]
     counts = [math.prod(sizes[axis] for axis in axes) for axes in groups]
 
     def members(axes):
@@ -171,18 +184,20 @@
     def first_pair(k, s):
         a, _ = mine(s)
         here = rows_of(k)
-        return remote(
-            part.at[s, 1 - a, :, :, here], first.at[s, :, :, here], rec_send.at[0], pair_recv.at[k, 0],
-            {"rep": partners[s]},
-        )
+        if kinds[k] == LATE:
+            source, target, sem = part.at[s, 1 - a, :, fs, here], first.at[s, :, 0, here], kind_send.at[0]
+        else:
+            source, target, sem = part.at[s, 1 - a, :, :, here], first.at[s, :, :, here], rec_send.at[0]
+        return remote(source, target, sem, pair_recv.at[k, 0], {"rep": partners[s]})
 
     def second_pair(k, s):
         a, b = mine(s)
         here = rows_of(k)
-        return remote(
-            part.at[s, a, 1 - b, fs, here], second.at[s, here], rec_send.at[2], pair_recv.at[k, 1],
-            {"rep": partners[1 - s]},
-        )
+        if kinds[k] == FINAL:
+            source, target, sem = part.at[s, a, 1 - b, :, here], thick_second.at[s, :, thick(k)], kind_send.at[1]
+        else:
+            source, target, sem = part.at[s, a, 1 - b, fs, here], second.at[s, here], rec_send.at[2]
+        return remote(source, target, sem, pair_recv.at[k, 1], {"rep": partners[1 - s]})
 
     def gather_pair(k, s, level):
         a, b = mine(s)
@@ -190,22 +205,42 @@
             here = grad.at[s, a, b, rows_of(k)]
         else:
             here = grad.at[s, a, :, rows_of(k)]
-        return remote(
-            here, here, rec_send.at[2], pair_recv.at[k, 2 + level], {"rep": partners[1 - s if level == 0 else s]}
-        )
+        sem = kind_send.at[2 + level] if kinds[k] == FINAL else rec_send.at[2]
+        return remote(here, here, sem, pair_recv.at[k, 2 + level], {"rep": partners[1 - s if level == 0 else s]})
+
+    def thick(k):
+        begin = units[k][3] - span_of(units, kinds, (FINAL,)).start
+        return slice(begin, begin + units[k][2] // 8)
 
     def chunk(k, s, owner):
         a, b = mine(s)
-        return gate_part.at[s, a, b, owner] if k == gate else part.at[s, a, :, owner, rows_of(k)]
+        if k == gate:
+            return gate_part.at[s, a, b, owner]
+        if kinds[k] == LATE:
+            return part.at[s, :, :, owner, rows_of(k)]
+        return part.at[s, a, b if kinds[k] == FINAL else slice(None), owner, rows_of(k)]
+
+    def ring_slots(k, s, steps):
+        if k == gate:
+            return gate_along.at[s, steps]
+        if kinds[k] == LATE:
+            return wide_along.at[s, steps, :, :, rows_of(k)]
+        return along.at[s, steps, 0 if kinds[k] == FINAL else slice(None), rows_of(k)]
 
     def ring_slot(k, s, step):
-        return gate_along.at[s, step - 1] if k == gate else along.at[s, step - 1, :, rows_of(k)]
+        return ring_slots(k, s, step - 1)
 
     def help_slot(k, s):
-        return gate_helped.at[s] if k == gate else helped.at[s, :, rows_of(k)]
+        if k == gate:
+            return gate_helped.at[s]
+        if kinds[k] == LATE:
+            return wide_helped.at[s, :, :, rows_of(k)]
+        return helped.at[s, 0 if kinds[k] == FINAL else slice(None), rows_of(k)]
 
     def ring_sem(k):
-        return gate_send.at[2] if k == gate else rec_send.at[1]
+        if k == gate:
+            return gate_send.at[2]
+        return rec_send.at[1] if kinds[k] == MIDDLE else kind_send.at[4 if kinds[k] == LATE else 5]
 
     def ring(k, s, step):
         peer = lax.rem(fs + step, fs_size)
@@ -254,7 +289,7 @@
     def fold(k):
         @pl.when(beside)
         def _():
-            arrived(gate_helped if k == gate else helped.at[:, :, rows_of(k)], help_recv.at[k])
+            arrived(help_slot(k, slice(None)), help_recv.at[k])
             for s in range(2):
                 whole = chunk(k, s, lax.rem(fs + fold_step, fs_size))
                 whole[...] += help_slot(k, s)[...]
@@ -262,7 +297,7 @@
 
     def ring_close(k):
         def slots_of(count):
-            return gate_along.at[:, 0:count] if k == gate else along.at[:, 0:count, :, rows_of(k)]
+            return ring_slots(k, slice(None), slice(0, count))
 
         pl.when(at_end)(lambda: arrived(slots_of(last - 1), ring_recv.at[k]))
         pl.when(jnp.logical_not(at_end))(lambda: arrived(slots_of(last), ring_recv.at[k]))
@@ -290,18 +325,23 @@
         if k == 0:
             pl.semaphore_wait(barrier, len(greeted))
         for s in range(2):
-            first_pair(k, s).start()
+            if kinds[k] == LATE:
+                ring_open(k, s)
+            else:
+                first_pair(k, s).start()
+
+    def add_first(k, s):
+        a, _ = mine(s)
+
+        @pl.loop(0, fs_size)
+        def _(owner):
+            for b in range(2):
+                part[s, a, b, owner, rows_of(k)] += first[s, b, owner, rows_of(k)]
 
     def spread(k):
         arrived(first.at[:, :, :, rows_of(k)], pair_recv.at[k, 0])
         for s in range(2):
-            a, _ = mine(s)
-
-            @pl.loop(0, fs_size)
-            def _(owner):
-                for b in range(2):
-                    part[s, a, b, owner, rows_of(k)] += first[s, b, owner, rows_of(k)]
-
+            add_first(k, s)
             ring_open(k, s)
 
     def collect(k):
@@ -309,15 +349,44 @@
         for s in range(2):
             second_pair(k, s).start()
 
+    def collect_late(k):
+        ring_close(k)
+        for s in range(2):
+            first_pair(k, s).start()
+
+    def add_late(k):
+        arrived(first.at[:, :, 0, rows_of(k)], pair_recv.at[k, 0])
+        for s in range(2):
+            a, _ = mine(s)
+            part[s, a, :, fs, rows_of(k)] += first[s, :, 0, rows_of(k)]
+            second_pair(k, s).start()
+
+    def halve(k):
+        arrived(first.at[:, :, :, rows_of(k)], pair_recv.at[k, 0])
+        for s in range(2):
+            add_first(k, s)
+            second_pair(k, s).start()
+
+    def spread_final(k):
+        arrived(thick_second.at[:, :, thick(k)], pair_recv.at[k, 1])
+        for s in range(2):
+            a, b = mine(s)
+            part[s, a, b, :, rows_of(k)] += thick_second[s, :, thick(k)]
+            ring_open(k, s)
+
     def settle(k):
         loaded("right", "moment")
-        arrived(second.at[:, rows_of(k)], pair_recv.at[k, 1])
+        if kinds[k] == FINAL:
+            ring_close(k)
+        else:
+            arrived(second.at[:, rows_of(k)], pair_recv.at[k, 1])
         _, start, size, _ = units[k]
         rows = size // 8
         gradients, moments = [], []
         for s in range(2):
             a, b = mine(s)
-            gradients.append(part[s, a, b, fs, rows_of(k)] + second[s, rows_of(k)])
+            quarter = part[s, a, b, fs, rows_of(k)]
+            gradients.append(quarter if kinds[k] == FINAL else quarter + second[s, rows_of(k)])
             begin = pl.multiple_of(start + (4 * s + 2 * a + b) * rows, 8)
             moments.append(rec_moment[pl.ds(begin, rows), column_of(k)])
         gradient = jnp.concatenate(gradients, axis=0)
@@ -480,7 +549,10 @@
             sums[3] += folded_squares(moment) * 0.25
 
     def rec_stages(k):
-        return [functools.partial(f, k) for f in (open_rec, spread, fold, collect, settle, forward, finish)]
+        middle = {
+            LATE: (fold, collect_late, add_late), MIDDLE: (spread, fold, collect), FINAL: (halve, spread_final, fold)
+        }[kinds[k]]
+        return [functools.partial(f, k) for f in (open_rec, *middle, settle, forward, finish)]
 
     gate_stages = [open_gate, gate_add_first]
     if by_head:
@@ -496,7 +568,8 @@
         offsets = GATE_AT if stages is gate_stages else REC_AT
         for stage, action in enumerate(stages):
             offset = offsets[stage] if stage < len(offsets) else offsets[-1] + stage + 1 - len(offsets)
-            agenda.append((max(0, place + offset), stage > 0, -place if stage else place, stage, action))
+            tick = OPEN_AT[place] if stage == 0 and place < len(OPEN_AT) else max(0, place + offset)
+            agenda.append((tick, stage > 0, -place if stage else place, stage, action))
 
     def exchange_open(index):
         axes, base = groups[index], sum(counts[:index])
@@ -527,11 +600,18 @@
                     message[i : i + 1] = jnp.sum(sums[i], axis=0, keepdims=True)
                 message[4:8] = jnp.zeros((4, LANES), jnp.float32)
                 exchange_open(0)
-
-    exchange_close(0)
+        elif left == 0:
+            exchange_close(0)
+            exchange_open(1)
+            left = None
+
+    if left is not None:
+        exchange_close(0)
+        exchange_open(1)
     for index in range(1, len(groups)):
-        exchange_open(index)
         exchange_close(index)
+        if index + 1 < len(groups):
+            exchange_open(index + 1)
     total = message[...]
     squares = [jnp.sum(total[i : i + 1], keepdims=True) for i in range(4)]
     rec_scale = jnp.sqrt(squares[0]) / jnp.sqrt(squares[1] + EPSILON)
@@ -539,9 +619,19 @@
     scales[0] = jnp.broadcast_to(rec_scale, (8, LANES))
     scales[1] = jnp.broadcast_to(gate_scale, (8, LANES))
 
-    sent(first, rec_send.at[0])
-    sent(along, rec_send.at[1])
-    sent(grad, rec_send.at[2])
+    early = span_of(units, kinds, (MIDDLE, FINAL))
+    sent(first.at[:, :, :, early], rec_send.at[0])
+    sent(along.at[:, :, :, span_of(units, kinds, (MIDDLE,))], rec_send.at[1])
+    sent(grad.at[:, :, :, span_of(units, kinds, (LATE, MIDDLE))], rec_send.at[2])
+    if LATE in kinds:
+        sent(first.at[:, :, 0, span_of(units, kinds, (LATE,))], kind_send.at[0])
+        sent(wide_along, kind_send.at[4])
+    if FINAL in kinds:
+        sent(thick_second, kind_send.at[1])
+        final = span_of(units, kinds, (FINAL,))
+        sent(grad.at[0, :, 0, final], kind_send.at[2])
+        sent(grad.at[0, :, :, final], kind_send.at[3])
+        sent(along.at[:, :, 0, final], kind_send.at[5])
     sent(gate_first, gate_send.at[0])
     sent(gate_second, gate_send.at[1])
     if by_head:
@@ -602,12 +692,13 @@
     fs_rows, columns = rec_weight.shape
     width = rec_right.shape[1]
     blocks, gate_rows = gate_weight.shape[:2]
-    units = plan(fs_rows, columns // width)
+    units, kinds = plan(fs_rows, columns // width)
+    late_span, final_span = span_of(units, kinds, (LATE,)), span_of(units, kinds, (FINAL,))
+    late, final = (span.stop - span.start if span else None for span in (late_span, final_span))
     rows = fs_rows * (columns // width) // 8
     others = fs_size - 1
     cubes = fs_size.bit_length() - 1
-    direct = fs_size * rep_size * tp_size <= 32
-    groups, tiles = (1, fs_size * rep_size * tp_size) if direct else (3, fs_size + rep_size + tp_size)
+    groups, tiles = (2, fs_size * tp_size + rep_size) if fs_size * tp_size <= 8 else (3, fs_size + tp_size + rep_size)
     loads = columns // width + sum(unit[0] == 0 for unit in units) + 7
     operands = (normed, rec_cot, conv_out, gate_cot, rec_moment, rec_right, gate_moment, gate_left, gate_right)
     vmem = pl.BlockSpec(memory_space=pltpu.VMEM)
@@ -629,7 +720,7 @@
         gate_grad = pltpu.VMEM((2, 2, 2, *piece), f32)
         gate_pre = None
     rec_new, gate_new, scales = pl.pallas_call(
-        functools.partial(kernel, fs_size, tp_size, units),
+        functools.partial(kernel, fs_size, tp_size, units, kinds),
         out_shape=(
             pltpu.VMEM(rec_weight.shape, f32),
             pltpu.VMEM(gate_weight.shape, f32),
@@ -645,6 +736,9 @@
             pltpu.VMEM((2, others, 2, rows, width), f32),
             pltpu.VMEM((2, 2, rows, width), f32),
             pltpu.VMEM((2, 2, 2, rows, width), f32),
+            late and pltpu.VMEM((2, others, 2, 2, late, width), f32),
+            late and pltpu.VMEM((2, 2, 2, late, width), f32),
+            final and pltpu.VMEM((2, fs_size, final, width), f32),
             pltpu.VMEM((2, 2, 2, *piece), f32),
             pltpu.VMEM((2, 2, *piece), f32),
             pltpu.VMEM((2, *piece), f32),
@@ -658,6 +752,7 @@
             pltpu.VMEM((tiles, 8, LANES), f32),
             dma((loads,)),
             dma((3,)),
+            dma((6,)),
             dma((len(units), 4)),
             dma((len(units) + 1,)),
             dma((len(units) + 1,)),

time: 109 us -> 102 us (0.936)
  Pallas kernels: 108 us -> 101 us
    pallas_call x1, Pallas kernels: 104 us -> 97.3 us  [shards(): pl.pallas_call(functools.partial(kernel, fs_size, tp_size, units, kinds),...]
where the time goes in v3:
time: 102 us; the launch traced here: 101 us
  Pallas kernels  101 us (99%)
    pallas_call x1, Pallas kernels, shards(): pl.pallas_call(functools.partial(kernel, fs_size, tp_size, units, kinds),...  97.3 us
    pallas_call x1, Pallas kernels, update(): pl.pallas_call(update_kernel, out_shape=shapes, in_specs=[vmem] * 5, out_...  3.5 us

profile of v3, /device:TPU:0, one launch (start us, length us, event | category | flops | bytes accessed | tf_op | source)
XLA Modules:
  0.0 101.5 jit_solution(7442180534543041471)
XLA Ops:
  0.6 0.0 copy-start.1
  0.6 0.0 copy-start
  0.7 97.3 %shard_map.170 = (f32[512,1024]{1,0:T(8,128)S(1)}, f32[4,64,256]{2,1,0:T(8,128)S(1)}, f32[2,8,128]{2,1,0:T(8,128)S(1)}) custom-call(bf16[640,2048]{1,0:T(8,128)(2,1)} %normed_hbm.1, bf16[640,1024]{1,0:T(8,128)(2,1)} %rec_cot_hbm.1, bf16[640,1024]{1,0:T(8,128)(2,1)} %conv_hbm.1, bf16[640,1024]{1,0:T(8,128)(2,1)} %gate_cot_hbm.1, f32[512,1024]{1,0:T(8,128)} %rec_moment_hbm.1, ...), custom_call_target="tpu_custom_call" | custom-call | tf_op jit(solution)/shard_map/pallas_call | solution.py:722
  98.0 0.0 copy-done.1
  98.0 0.0 copy-done
  98.0 3.5 %shard_map.171 = (f32[512,1024]{1,0:T(8,128)}, f32[512,1024]{1,0:T(8,128)}, f32[512,1024]{1,0:T(8,128)}, bf16[512,1024]{1,0:T(8,128)(2,1)}, f32[4,64,256]{2,1,0:...) custom-call(f32[512,1024]{1,0:T(8,128)S(1)} %copy-done, ...), custom_call_target="tpu_custom_call" | custom-call | tf_op jit(solution)/shard_map/pallas_call | solution.py:783
Async XLA Ops:
  0.6 97.3 %copy-start.1 = (f32[4,64,256]{2,1,0:T(8,128)S(1)}, f32[4,64,256]{2,1,0:T(8,128)}, u32[]{:S(2)}) copy-start(f32[4,64,256]{2,1,0:T(8,128)} %gate_weight.1) | copy-start | bytes 786436
  0.6 97.3 %copy-start = (f32[512,1024]{1,0:T(8,128)S(1)}, f32[512,1024]{1,0:T(8,128)}, u32[]{:S(2)}) copy-start(f32[512,1024]{1,0:T(8,128)} %rec_weight.1) | copy-start | bytes 6291460

commit v4 on v3

--- a/solution.py
+++ b/solution.py
@@ -283,7 +283,7 @@
 
     def ring_open(k, s):
         pl.when(at_end)(lambda: helper(k, s).start())
-        for step in range(1, fs_size):
+        for step in sorted(range(1, fs_size), key=lambda step: -min(step, fs_size - step)):
             when(sends(step), lambda step=step: ring(k, s, step).start())
 
     def fold(k):

time: 102 us -> 102 us (level)
  no operation moved by 1% of the time
where the time goes in v4:
time: 102 us; the launch traced here: 101 us
  Pallas kernels  101 us (99%)
    pallas_call x1, Pallas kernels, shards(): pl.pallas_call(functools.partial(kernel, fs_size, tp_size, units, kinds),...  97.3 us
    pallas_call x1, Pallas kernels, update(): pl.pallas_call(update_kernel, out_shape=shapes, in_specs=[vmem] * 5, out_...  3.5 us

profile of v4, /device:TPU:0, one launch (start us, length us, event | category | flops | bytes accessed | tf_op | source)
XLA Modules:
  0.0 101.5 jit_solution(8500784300924998260)
XLA Ops:
  0.6 0.0 copy-start.1
  0.6 0.0 copy-start
  0.7 97.3 %shard_map.170 = (f32[512,1024]{1,0:T(8,128)S(1)}, f32[4,64,256]{2,1,0:T(8,128)S(1)}, f32[2,8,128]{2,1,0:T(8,128)S(1)}) custom-call(bf16[640,2048]{1,0:T(8,128)(2,1)} %normed_hbm.1, bf16[640,1024]{1,0:T(8,128)(2,1)} %rec_cot_hbm.1, bf16[640,1024]{1,0:T(8,128)(2,1)} %conv_hbm.1, bf16[640,1024]{1,0:T(8,128)(2,1)} %gate_cot_hbm.1, f32[512,1024]{1,0:T(8,128)} %rec_moment_hbm.1, ...), custom_call_target="tpu_custom_call" | custom-call | tf_op jit(solution)/shard_map/pallas_call | solution.py:722
  98.0 0.0 copy-done.1
  98.0 0.0 copy-done
  98.0 3.5 %shard_map.171 = (f32[512,1024]{1,0:T(8,128)}, f32[512,1024]{1,0:T(8,128)}, f32[512,1024]{1,0:T(8,128)}, bf16[512,1024]{1,0:T(8,128)(2,1)}, f32[4,64,256]{2,1,0:...) custom-call(f32[512,1024]{1,0:T(8,128)S(1)} %copy-done, ...), custom_call_target="tpu_custom_call" | custom-call | tf_op jit(solution)/shard_map/pallas_call | solution.py:783
Async XLA Ops:
  0.6 97.3 %copy-start.1 = (f32[4,64,256]{2,1,0:T(8,128)S(1)}, f32[4,64,256]{2,1,0:T(8,128)}, u32[]{:S(2)}) copy-start(f32[4,64,256]{2,1,0:T(8,128)} %gate_weight.1) | copy-start | bytes 786436
  0.6 97.3 %copy-start = (f32[512,1024]{1,0:T(8,128)S(1)}, f32[512,1024]{1,0:T(8,128)}, u32[]{:S(2)}) copy-start(f32[512,1024]{1,0:T(8,128)} %rec_weight.1) | copy-start | bytes 6291460
